TPU v7x, 32 devices: a whole 2x2x4 slice. The times are simulated.
32 devices in a mesh: sp: 8 (over z, core), tp: 4 (over y, x).
Axes of the slice: x: 2, y: 2, z: 4, core: 2. Of those that a mesh axis runs over, the one named last changes fastest.
Arguments:
- residual: bfloat16 [3072, 2048], P('sp', 'tp'), may hold values from -40 to 40
- norm_gain: bfloat16 [3, 2048], P(None, 'tp'), may hold values from 0.099609375 to 1.8984375
- w_query: bfloat16 [3, 2048, 2048], P(None, 'tp'), may hold values from -2 to 2
- w_key: bfloat16 [3, 2048, 2048], P(None, 'tp'), may hold values from -8 to 8
- w_value: bfloat16 [3, 2048, 2048], P(None, 'tp'), may hold values from -0.125 to 0.125
- w_out: bfloat16 [3, 2048, 2048], P(None, 'tp'), may hold values from -0.25 to 0.25
- offset_bias: float32 [3, 32, 15, 31], P(None, 'tp'), may hold values from -5 to 5
Outputs:
- out_residual: bfloat16 [3072, 2048], P('sp', 'tp')
All inputs are finite; a program needn't handle non-finite values.
Results may differ from a plain program's by a relative error of at most 0.014.
Values may be sent and summed in bfloat16 or wider, within the bound.
A program may use at most 128 MiB of HBM per device.

v0:
```python
import jax
import jax.numpy as jnp
from jax import lax
from jax.experimental import pallas as pl
from jax.experimental.pallas import tpu as pltpu
from jax.sharding import PartitionSpec as P

HEAD_DIM = 64
GRID_W = 64
NA_ROWS = 8
NA_COLS = 16
LAYERS = 3


epsilon = 1e-06


def padded_2(array, sides, width):
    for axis, dim in sides:
        size, length = (lax.axis_size(axis), array.shape[dim])
        up = [(i, (i + 1) % size) for i in range(size - 1)]
        down = [(j, i) for i, j in up]
        last = lax.slice_in_dim(array, length - width, length, axis=dim)
        first = lax.slice_in_dim(array, 0, width, axis=dim)
        before = lax.ppermute(last, axis, up)
        after = lax.ppermute(first, axis, down)
        array = jnp.concatenate([before, array, after], axis=dim)
    return array


def shortened(array):
    return jax.tree.map(lambda a: a.astype(jnp.bfloat16) if a.dtype == jnp.float32 else a, array)


def contract(left, right):
    return lax.dot_general(
        left, right, (((1,), (1,)), ((), ())), preferred_element_type=jnp.float32
    )


def generic_device(residual, norm_gain, w_query, w_key, w_value, w_out, offset_bias):
    token_count = residual.shape[0]
    local_feats = residual.shape[1]
    local_heads = offset_bias.shape[1]
    head_cols = local_heads * HEAD_DIM
    rows_dev = token_count // GRID_W
    rows_all = rows_dev * lax.axis_size("sp")
    row_base = lax.axis_index("sp") * rows_dev
    reach = NA_ROWS // 2
    slab_width = min(2 * NA_COLS, GRID_W)
    tile_starts = list(range(0, GRID_W, NA_COLS))
    slab_starts = [min(max(start - NA_COLS // 2, 0), GRID_W - slab_width) for start in tile_starts]
    tile_info = []
    for start, slab in zip(tile_starts, slab_starts):
        query_cols = start + jnp.arange(NA_COLS, dtype=jnp.int32)
        key_cols = slab + jnp.arange(slab_width, dtype=jnp.int32)
        first_col = jnp.clip(query_cols - NA_COLS // 2, 0, GRID_W - NA_COLS)
        inside = (key_cols[None, :] >= first_col[:, None]) & (
            key_cols[None, :] < first_col[:, None] + NA_COLS
        )
        offsets = key_cols[None, :] - query_cols[:, None] + (NA_COLS - 1)
        onehot = (offsets[:, :, None] == jnp.arange(2 * NA_COLS - 1, dtype=jnp.int32)).astype(
            jnp.float32
        )
        tile_info.append((start, slab, inside, onehot))
    stream = residual
    for layer_index in range(LAYERS):
        res_float = stream.astype(jnp.float32)
        gathered, gain_all = (
            lax.all_gather(stream, "tp", axis=1, tiled=True),
            lax.all_gather(norm_gain[layer_index][None, :], "tp", axis=1, tiled=True),
        )
        full_float = gathered.astype(jnp.float32)
        inverse = lax.rsqrt(jnp.mean(full_float * full_float, axis=1, keepdims=True) + epsilon)
        normed_all = (full_float * inverse * gain_all.astype(jnp.float32)).astype(jnp.bfloat16)
        queries = contract(normed_all, w_query[layer_index])
        keys = contract(normed_all, w_key[layer_index])
        values = contract(normed_all, w_value[layer_index])
        queries = queries.astype(jnp.bfloat16)
        key_value = jnp.concatenate(
            [keys.astype(jnp.bfloat16), values.astype(jnp.bfloat16)], axis=1
        )
        padded = padded_2(key_value, (("sp", 0),), reach * GRID_W)
        key_grid = padded.reshape(rows_dev + 2 * reach, GRID_W, 2, local_heads, HEAD_DIM)
        query_grid = queries.reshape(rows_dev, GRID_W, local_heads, HEAD_DIM)
        lookup = offset_bias[layer_index]

        def one_row(row_index, query_row):
            row_global = row_base + row_index
            first_row = jnp.clip(row_global - reach, 0, rows_all - NA_ROWS)
            local_first = first_row - row_base + reach
            window = lax.dynamic_slice_in_dim(key_grid, local_first, NA_ROWS, 0)
            row_offset = (
                first_row + jnp.arange(NA_ROWS, dtype=jnp.int32) - row_global + (NA_ROWS - 1)
            )
            row_onehot = (
                row_offset[:, None] == jnp.arange(2 * NA_ROWS - 1, dtype=jnp.int32)
            ).astype(jnp.float32)
            row_bias = jnp.einsum(
                "hab,ra->hrb", lookup, row_onehot, precision=lax.Precision.HIGHEST
            )
            pieces = []
            for start, slab, inside, onehot in tile_info:
                query_tile = query_row[start : start + NA_COLS]
                slab_keys = window[:, slab : slab + slab_width, 0]
                slab_values = window[:, slab : slab + slab_width, 1]
                bias_terms = jnp.einsum(
                    "hrb,wsb->hwrs", row_bias, onehot, precision=lax.Precision.HIGHEST
                )
                scores = jnp.einsum(
                    "whd,rshd->hwrs", query_tile, slab_keys, preferred_element_type=jnp.float32
                )
                scores = scores * HEAD_DIM ** (-0.5) + bias_terms
                scores = jnp.where(inside[None, :, None, :], scores, -jnp.inf)
                weights = jax.nn.softmax(
                    scores.reshape(local_heads, NA_COLS, NA_ROWS * slab_width), axis=-1
                ).astype(jnp.bfloat16)
                weights = weights.reshape(local_heads, NA_COLS, NA_ROWS, slab_width)
                attended = jnp.einsum(
                    "hwrs,rshd->whd", weights, slab_values, preferred_element_type=jnp.float32
                )
                pieces.append(attended.astype(jnp.bfloat16).reshape(NA_COLS, head_cols))
            return jnp.concatenate(pieces, axis=0)

        attended = jax.vmap(one_row)(jnp.arange(rows_dev, dtype=jnp.int32), query_grid).reshape(
            token_count, head_cols
        )
        portion = jax.tree.map(
            lambda part: lax.all_gather(part, "tp", axis=1, tiled=True), shortened(attended)
        )
        out_rows = lax.slice_in_dim(w_out[layer_index], 0, portion.shape[1], axis=1)
        mixed = jnp.zeros((token_count, local_feats), jnp.float32) + contract(portion, out_rows)
        stream = (res_float + mixed).astype(jnp.bfloat16)
    return stream


def bias_lanes(offset_bias):
    layers, heads, row_offs, col_offs = offset_bias.shape
    flipped = jnp.flip(offset_bias, axis=3)
    padded = jnp.pad(flipped, ((0, 0), (0, 0), (0, 1), (0, GRID_W - col_offs)))
    paired = padded.reshape(layers, heads // 2, 2, row_offs + 1, GRID_W)
    return paired.transpose(0, 1, 3, 2, 4).reshape(layers, heads // 2, row_offs + 1, 2 * GRID_W)


def window_mask():
    shape = (GRID_W, 2 * GRID_W)
    key_col = lax.broadcasted_iota(jnp.int32, shape, 0)
    query_col = lax.broadcasted_iota(jnp.int32, shape, 1) % GRID_W
    first = jnp.clip(query_col - NA_COLS // 2, 0, GRID_W - NA_COLS)
    return (key_col >= first) & (key_col < first + NA_COLS)


def build_table(lanes_of, table):
    inside = window_mask()
    for off in range(2 * NA_ROWS - 1):
        row = jnp.broadcast_to(lanes_of(off), (GRID_W, 2 * GRID_W))
        rolled = pltpu.roll(row, 2 * GRID_W - (NA_COLS - 1), axis=1, stride=1, stride_axis=0)
        table[off * GRID_W : (off + 1) * GRID_W, :] = jnp.where(inside, rolled, -1e30)


def attend_row(query, window_keys, window_values, bias):
    low = lax.broadcasted_iota(jnp.int32, query.shape, 1) < HEAD_DIM
    zero = jnp.zeros_like(query)
    block = jnp.concatenate([jnp.where(low, query, zero), jnp.where(low, zero, query)], axis=0)
    scores = contract(window_keys, block) + bias
    top = jnp.max(scores, axis=0, keepdims=True)
    weights = jnp.exp(scores - top)
    inverse = 1.0 / jnp.sum(weights, axis=0, keepdims=True)
    weights = (weights * inverse).astype(jnp.bfloat16)
    mixed = lax.dot_general(
        weights, window_values, (((0,), (0,)), ((), ())), preferred_element_type=jnp.float32
    )
    return jnp.where(low, mixed[:GRID_W], mixed[GRID_W:]).astype(jnp.bfloat16)


def row_window(row, rows_dev, rows_all):
    reach = NA_ROWS // 2
    row_base = lax.axis_index("sp") * rows_dev
    first = jnp.clip(row_base + row - reach, 0, rows_all - NA_ROWS)
    return first - row_base + reach, first - row_base - row + NA_ROWS - 1


MESH = pl.DeviceIdType.MESH
LAG = 3


def tp_copy(src, dst, sems, index, peer):
    return pltpu.make_async_remote_copy(
        src_ref=src,
        dst_ref=dst,
        send_sem=sems.at[0, index],
        recv_sem=sems.at[1, index],
        device_id=(lax.axis_index("sp"), peer),
        device_id_type=MESH,
    )


class SquareGather:
    def __init__(self, slots, sems, chunks):
        self.slots, self.sems, self.chunks = slots, sems, chunks
        self.rows = slots.shape[1] // chunks
        self.me = lax.axis_index("tp")
        self.across = self.me + 1 - 2 * (self.me % 2)
        self.over = (self.me + 2) % 4
        self.corner = (self.across + 2) % 4

    def part(self, slot, chunk):
        start = chunk * self.rows
        if not isinstance(chunk, int):
            start = pl.multiple_of(start, self.rows)
        return self.slots.at[slot, pl.ds(start, self.rows), :]

    def copy(self, kind, slot, chunk, peer):
        part = self.part(slot, chunk)
        return tp_copy(part, part, self.sems.at[kind], chunk, peer)

    def send(self, chunk):
        self.copy(0, self.me, chunk, self.across).start()
        self.copy(1, self.me, chunk, self.over).start()

    def relay(self, chunk):
        self.copy(0, self.across, chunk, self.across).wait_recv()
        self.copy(1, self.over, chunk, self.over).wait_recv()

        @pl.when(chunk % 2 == 0)
        def _():
            self.copy(2, self.across, chunk, self.over).start()

        @pl.when(chunk % 2 == 1)
        def _():
            self.copy(2, self.over, chunk, self.across).start()

    def finish(self, chunk):
        self.copy(2, self.corner, chunk, self.over).wait_recv()

    def drain(self):
        def one(chunk, carry):
            self.copy(0, self.me, chunk, self.across).wait_send()
            self.copy(1, self.me, chunk, self.over).wait_send()
            self.copy(2, self.across, chunk, self.over).wait_send()
            return carry

        lax.fori_loop(0, self.chunks, one, 0)


def stack_kernel(
    rows_dev, rows_all,
    x_ref, gain_ref, lanes_ref, wq_ref, wk_ref, wv_ref, wo_ref, out_ref,
    gains, weights, stream, mixed, keyval, queries, normed, tables,
    partial, weight_sems, gain_sems, stream_sems, mixed_sems, halo_sems,
):
    sp, sp_size = lax.axis_index("sp"), lax.axis_size("sp")
    layers = wq_ref.shape[0]
    tokens, feats = x_ref.shape
    width = feats
    reach = NA_ROWS // 2 * GRID_W
    streams = SquareGather(stream, stream_sems, rows_dev)
    mixes = SquareGather(mixed, mixed_sems, rows_dev)
    me, across, over = streams.me, streams.across, streams.over
    corner = streams.corner
    sources = (wk_ref, wv_ref, wq_ref, wo_ref)

    def weight_copy(kind, layer):
        return pltpu.make_async_copy(
            sources[kind].at[layer], weights.at[kind, layer], weight_sems.at[kind, layer]
        )

    for layer in range(layers):
        for kind in range(4):
            weight_copy(kind, layer).start()

    barrier = pltpu.get_barrier_semaphore()
    for peer in (across, over, corner):
        pl.semaphore_signal(barrier, inc=1, device_id=(sp, peer), device_id_type=MESH)

    @pl.when(sp > 0)
    def _():
        pl.semaphore_signal(barrier, inc=1, device_id=(sp - 1, me), device_id_type=MESH)

    @pl.when(sp < sp_size - 1)
    def _():
        pl.semaphore_signal(barrier, inc=1, device_id=(sp + 1, me), device_id_type=MESH)

    stream[me] = x_ref[...]
    gains[me, 0:layers, :] = gain_ref[...].astype(jnp.float32)
    sides = jnp.minimum(sp, 1) + jnp.minimum(sp_size - 1 - sp, 1)
    pl.semaphore_wait(barrier, 3 + sides)

    def gain_copy(index, slot, peer):
        return tp_copy(gains.at[slot], gains.at[slot], gain_sems, index, peer)

    for index, peer in enumerate((across, over, corner)):
        gain_copy(index, me, peer).start()

    pairs = rows_dev // 2
    tall = 2 * GRID_W
    parts = NA_ROWS // 4
    down_parts = range(parts)
    up_parts = range(pairs - parts, pairs)
    order = sorted(range(pairs), key=lambda j: -((j in down_parts) + (j in up_parts)))

    def halo_copy(parity, up, part, kind):
        cols = slice(kind * width, (kind + 1) * width)
        local = reach + (pairs - parts + part if up else part) * tall
        there = part * tall + (0 if up else tokens + reach)
        return pltpu.make_async_remote_copy(
            src_ref=keyval.at[parity, pl.ds(local, tall), cols],
            dst_ref=keyval.at[parity, pl.ds(there, tall), cols],
            send_sem=halo_sems.at[0, parity, int(up), part, kind],
            recv_sem=halo_sems.at[1, parity, int(up), part, kind],
            device_id=(sp + 1 if up else sp - 1, me),
            device_id_type=MESH,
        )

    def send_halo(parity, pair, kind):
        if pair in down_parts:

            @pl.when(sp > 0)
            def _():
                halo_copy(parity, False, pair, kind).start()

        if pair in up_parts:

            @pl.when(sp < sp_size - 1)
            def _():
                halo_copy(parity, True, pair - (pairs - parts), kind).start()

    def one_layer(layer, carry):
        parity = layer % 2
        for pair in order[:2]:
            streams.send(2 * pair)
            streams.send(2 * pair + 1)
        for pair in range(width // 128):
            build_table(
                lambda off: lanes_ref[layer, pair, off : off + 1, :], tables.at[pair]
            )

        def relay_pair(pair):
            streams.relay(2 * pair)
            streams.relay(2 * pair + 1)

        def norm_pair(pair):
            here = slice(pair * tall, (pair + 1) * tall)
            total = jnp.zeros((tall, 1), jnp.float32)
            for slot in range(4):
                part = stream[slot, here, :].astype(jnp.float32)
                total += jnp.sum(part * part, axis=1, keepdims=True)
            inverse = lax.rsqrt(total * (1.0 / (4 * feats)) + epsilon)
            for slot in range(4):
                part = stream[slot, here, :].astype(jnp.float32)
                gain = gains[slot, pl.ds(layer, 1), :]
                normed[here, slot * feats : (slot + 1) * feats] = (
                    part * inverse * gain
                ).astype(jnp.bfloat16)

        def project_pair(pair):
            here = slice(pair * tall, (pair + 1) * tall)
            there = slice(reach + pair * tall, reach + (pair + 1) * tall)
            for kind in range(2):
                keyval[parity, there, kind * width : (kind + 1) * width] = contract(
                    normed[here, :], weights[kind, layer]
                ).astype(jnp.bfloat16)
                send_halo(parity, pair, kind)
            queries[here, :] = contract(normed[here, :], weights[2, layer]).astype(
                jnp.bfloat16
            ) * jnp.bfloat16(HEAD_DIM ** (-0.5))

        @pl.when(layer == 0)
        def _():
            for index, peer in enumerate((across, over, corner)):
                gain_copy(index, peer, peer).wait_recv()
                gain_copy(index, me, peer).wait_send()

        for kind in range(3):
            weight_copy(kind, layer).wait()
        relay_pair(order[0])
        for pair in order[2:]:
            streams.send(2 * pair)
            streams.send(2 * pair + 1)
        for place, pair in enumerate(order):
            if place + 1 < pairs:
                relay_pair(order[place + 1])
            streams.finish(2 * pair)
            streams.finish(2 * pair + 1)
            norm_pair(pair)
            project_pair(pair)
        streams.drain()

        def wait_halo(up):
            for part in range(parts):
                for kind in range(2):
                    halo_copy(parity, up, part, kind).wait_recv()

        @pl.when(sp < sp_size - 1)
        def _():
            wait_halo(False)

        @pl.when((sp > 0) & (sp == sp_size - 1))
        def _():
            wait_halo(True)

        def one_row(step, carry):
            row = rows_dev - 1 - step

            @pl.when((step == rows_dev - NA_ROWS // 2) & (sp > 0) & (sp < sp_size - 1))
            def _():
                wait_halo(True)

            start, off = row_window(row, rows_dev, rows_all)
            keys = pl.ds(pl.multiple_of(start * GRID_W, GRID_W), NA_ROWS * GRID_W)
            here = pl.ds(pl.multiple_of(row * GRID_W, GRID_W), GRID_W)
            offs = pl.ds(pl.multiple_of(off * GRID_W, GRID_W), NA_ROWS * GRID_W)
            for pair in range(width // 128):
                cols = slice(pair * 128, (pair + 1) * 128)
                vcols = slice(width + pair * 128, width + (pair + 1) * 128)
                mixed[me, here, cols] = attend_row(
                    queries[here, cols],
                    keyval[parity, keys, cols],
                    keyval[parity, keys, vcols],
                    tables[pair, offs, :],
                )
            mixes.send(row)

            @pl.when(step >= LAG)
            def _():
                mixes.relay(row + LAG)

            return carry

        lax.fori_loop(0, rows_dev, one_row, 0)

        def relay_rest(step, carry):
            mixes.relay(rows_dev - 1 - step)
            return carry

        lax.fori_loop(rows_dev - LAG, rows_dev, relay_rest, 0)
        weight_copy(3, layer).wait()

        def out_part(slot):
            cols = pl.ds(pl.multiple_of(slot * width, width), width)
            return contract(mixed[slot], weights[3, layer, :, cols])

        total = stream[me].astype(jnp.float32) + out_part(me)
        partial[...] = total + out_part(across) + out_part(over)

        for part in range(parts):
            for kind in range(2):

                @pl.when(sp > 0)
                def _():
                    halo_copy(parity, False, part, kind).wait_send()

                @pl.when(sp < sp_size - 1)
                def _():
                    halo_copy(parity, True, part, kind).wait_send()

        def finish_chunk(chunk, carry):
            mixes.finish(chunk)
            return carry

        lax.fori_loop(0, rows_dev, finish_chunk, 0)
        mixes.drain()
        total = partial[...] + out_part(corner)
        stream[me] = total.astype(jnp.bfloat16)
        return carry

    lax.fori_loop(0, layers, one_layer, 0)
    out_ref[...] = stream[me]


def square_device(residual, norm_gain, w_query, w_key, w_value, w_out, offset_bias):
    tokens, feats = residual.shape
    layers = w_query.shape[0]
    rows_dev = tokens // GRID_W
    rows_all = rows_dev * lax.axis_size("sp")
    lanes = bias_lanes(offset_bias)
    vmem = pl.BlockSpec(memory_space=pltpu.VMEM)
    hbm = pl.BlockSpec(memory_space=pl.ANY)
    bf16, dma = jnp.bfloat16, pltpu.SemaphoreType.DMA
    padded = tokens + NA_ROWS * GRID_W
    return pl.pallas_call(
        lambda *refs: stack_kernel(rows_dev, rows_all, *refs),
        out_shape=jax.ShapeDtypeStruct(residual.shape, bf16),
        in_specs=[vmem] * 3 + [hbm] * 4,
        out_specs=vmem,
        scratch_shapes=[
            pltpu.VMEM((4, -(-layers // 8) * 8, feats), jnp.float32),
            pltpu.VMEM((4,) + w_query.shape, bf16),
            pltpu.VMEM((4, tokens, feats), bf16),
            pltpu.VMEM((4, tokens, feats), bf16),
            pltpu.VMEM((2, padded, 2 * feats), bf16),
            pltpu.VMEM((tokens, feats), bf16),
            pltpu.VMEM((tokens, 4 * feats), bf16),
            pltpu.VMEM((feats // 128, (2 * NA_ROWS - 1) * GRID_W, 128), jnp.float32),
            pltpu.VMEM((tokens, feats), jnp.float32),
            dma((4, layers)),
            dma((2, 3)),
            dma((3, 2, rows_dev)),
            dma((3, 2, rows_dev)),
            dma((2, 2, 2, NA_ROWS // 4, 2)),
        ],
        compiler_params=pltpu.CompilerParams(
            collective_id=0, has_side_effects=True, vmem_limit_bytes=56 * 1024 * 1024
        ),
        name="stack",
    )(residual, norm_gain, lanes, w_query, w_key, w_value, w_out)


def per_device(residual, norm_gain, w_query, w_key, w_value, w_out, offset_bias):
    paired = offset_bias.shape[1] % 2 == 0 and 2 * HEAD_DIM == 128 and 2 * GRID_W == 128
    square = lax.axis_size("tp") == 4 and offset_bias.shape[1] * HEAD_DIM == residual.shape[1]
    rows_dev = residual.shape[0] // GRID_W
    even = rows_dev % 2 == 0 and rows_dev >= NA_ROWS // 2
    body = generic_device
    if paired and square and even:
        body = square_device
    return body(residual, norm_gain, w_query, w_key, w_value, w_out, offset_bias)


def solution(mesh):
    in_specs = (
        P("sp", "tp"),
        P(None, "tp"),
        P(None, "tp", None),
        P(None, "tp", None),
        P(None, "tp", None),
        P(None, "tp", None),
        P(None, "tp", None, None),
    )
    out_specs = P("sp", "tp")
    return jax.shard_map(
        per_device, mesh=mesh, in_specs=in_specs, out_specs=out_specs, check_vma=False
    )
```

profile of v0, /device:TPU:8, one launch (start us, length us, event | category | flops | bytes accessed | tf_op | source)
XLA Modules:
  0.0 116.5 jit_solution(17833300808582484427)
XLA Ops:
  0.0 1.0 rev.4
  1.1 0.1 copy.10
  1.2 0.8 reshape.7.refs_2_
  2.0 112.7 %stack.1 = bf16[384,512]{1,0:T(8,128)(2,1)} custom-call(bf16[384,512]{1,0:T(8,128)(2,1)} %refs_0_.1, bf16[3,512]{1,0:T(4,128)(2,1)} %refs_1_.1, f32[3,4,16,128]{3,2,1,0:T(8,128)} %reshape.7.refs_2_, bf16[3,512,2048]{2,1,0:T(8,128)(2,1)} %refs_3_.1, bf16[3,512,2048]{2,1,0:T(8,128)(2,1)} %refs_4_.1, bf16[3,512,2048]{2,1,0:T(8,128)(2,1)} %refs_5_.1, ...), custom_call_target="tpu_custom_call" | custom-call | tf_op jit(solution)/shard_map/stack/pallas_call | solution.py:481
  114.7 1.8 %copy.12 = bf16[384,512]{1,0:T(8,128)(2,1)} copy(bf16[384,512]{1,0:T(8,128)(2,1)} %stack.1) | data formatting | bytes 786432
  (1 shorter events, 0.0 us)
where the time goes:
time: 118 us; the launch traced here: 116 us
  Pallas kernels  113 us (96%)
  local copies, waits for them, and re-layouts  3.69 us (3%)
    pallas_call x1, Pallas kernels, square_device(): pl.pallas_call(lambda *refs: stack_kernel(rows_dev, rows_all, *refs), out...  113 us

commit v1 on v0

v1 whole, which is shorter than its diff:
```python
import jax
import jax.numpy as jnp
from jax import lax
from jax.experimental import pallas as pl
from jax.experimental.pallas import tpu as pltpu
from jax.sharding import PartitionSpec as P

HEAD_DIM = 64
GRID_W = 64
NA_ROWS = 8
NA_COLS = 16
LAYERS = 3


epsilon = 1e-06


def padded_2(array, sides, width):
    for axis, dim in sides:
        size, length = (lax.axis_size(axis), array.shape[dim])
        up = [(i, (i + 1) % size) for i in range(size - 1)]
        down = [(j, i) for i, j in up]
        last = lax.slice_in_dim(array, length - width, length, axis=dim)
        first = lax.slice_in_dim(array, 0, width, axis=dim)
        before = lax.ppermute(last, axis, up)
        after = lax.ppermute(first, axis, down)
        array = jnp.concatenate([before, array, after], axis=dim)
    return array


def shortened(array):
    return jax.tree.map(lambda a: a.astype(jnp.bfloat16) if a.dtype == jnp.float32 else a, array)


def contract(left, right):
    return lax.dot_general(
        left, right, (((1,), (1,)), ((), ())), preferred_element_type=jnp.float32
    )


def generic_device(residual, norm_gain, w_query, w_key, w_value, w_out, offset_bias):
    token_count = residual.shape[0]
    local_feats = residual.shape[1]
    local_heads = offset_bias.shape[1]
    head_cols = local_heads * HEAD_DIM
    rows_dev = token_count // GRID_W
    rows_all = rows_dev * lax.axis_size("sp")
    row_base = lax.axis_index("sp") * rows_dev
    reach = NA_ROWS // 2
    slab_width = min(2 * NA_COLS, GRID_W)
    tile_starts = list(range(0, GRID_W, NA_COLS))
    slab_starts = [min(max(start - NA_COLS // 2, 0), GRID_W - slab_width) for start in tile_starts]
    tile_info = []
    for start, slab in zip(tile_starts, slab_starts):
        query_cols = start + jnp.arange(NA_COLS, dtype=jnp.int32)
        key_cols = slab + jnp.arange(slab_width, dtype=jnp.int32)
        first_col = jnp.clip(query_cols - NA_COLS // 2, 0, GRID_W - NA_COLS)
        inside = (key_cols[None, :] >= first_col[:, None]) & (
            key_cols[None, :] < first_col[:, None] + NA_COLS
        )
        offsets = key_cols[None, :] - query_cols[:, None] + (NA_COLS - 1)
        onehot = (offsets[:, :, None] == jnp.arange(2 * NA_COLS - 1, dtype=jnp.int32)).astype(
            jnp.float32
        )
        tile_info.append((start, slab, inside, onehot))
    stream = residual
    for layer_index in range(LAYERS):
        res_float = stream.astype(jnp.float32)
        gathered, gain_all = (
            lax.all_gather(stream, "tp", axis=1, tiled=True),
            lax.all_gather(norm_gain[layer_index][None, :], "tp", axis=1, tiled=True),
        )
        full_float = gathered.astype(jnp.float32)
        inverse = lax.rsqrt(jnp.mean(full_float * full_float, axis=1, keepdims=True) + epsilon)
        normed_all = (full_float * inverse * gain_all.astype(jnp.float32)).astype(jnp.bfloat16)
        queries = contract(normed_all, w_query[layer_index])
        keys = contract(normed_all, w_key[layer_index])
        values = contract(normed_all, w_value[layer_index])
        queries = queries.astype(jnp.bfloat16)
        key_value = jnp.concatenate(
            [keys.astype(jnp.bfloat16), values.astype(jnp.bfloat16)], axis=1
        )
        padded = padded_2(key_value, (("sp", 0),), reach * GRID_W)
        key_grid = padded.reshape(rows_dev + 2 * reach, GRID_W, 2, local_heads, HEAD_DIM)
        query_grid = queries.reshape(rows_dev, GRID_W, local_heads, HEAD_DIM)
        lookup = offset_bias[layer_index]

        def one_row(row_index, query_row):
            row_global = row_base + row_index
            first_row = jnp.clip(row_global - reach, 0, rows_all - NA_ROWS)
            local_first = first_row - row_base + reach
            window = lax.dynamic_slice_in_dim(key_grid, local_first, NA_ROWS, 0)
            row_offset = (
                first_row + jnp.arange(NA_ROWS, dtype=jnp.int32) - row_global + (NA_ROWS - 1)
            )
            row_onehot = (
                row_offset[:, None] == jnp.arange(2 * NA_ROWS - 1, dtype=jnp.int32)
            ).astype(jnp.float32)
            row_bias = jnp.einsum(
                "hab,ra->hrb", lookup, row_onehot, precision=lax.Precision.HIGHEST
            )
            pieces = []
            for start, slab, inside, onehot in tile_info:
                query_tile = query_row[start : start + NA_COLS]
                slab_keys = window[:, slab : slab + slab_width, 0]
                slab_values = window[:, slab : slab + slab_width, 1]
                bias_terms = jnp.einsum(
                    "hrb,wsb->hwrs", row_bias, onehot, precision=lax.Precision.HIGHEST
                )
                scores = jnp.einsum(
                    "whd,rshd->hwrs", query_tile, slab_keys, preferred_element_type=jnp.float32
                )
                scores = scores * HEAD_DIM ** (-0.5) + bias_terms
                scores = jnp.where(inside[None, :, None, :], scores, -jnp.inf)
                weights = jax.nn.softmax(
                    scores.reshape(local_heads, NA_COLS, NA_ROWS * slab_width), axis=-1
                ).astype(jnp.bfloat16)
                weights = weights.reshape(local_heads, NA_COLS, NA_ROWS, slab_width)
                attended = jnp.einsum(
                    "hwrs,rshd->whd", weights, slab_values, preferred_element_type=jnp.float32
                )
                pieces.append(attended.astype(jnp.bfloat16).reshape(NA_COLS, head_cols))
            return jnp.concatenate(pieces, axis=0)

        attended = jax.vmap(one_row)(jnp.arange(rows_dev, dtype=jnp.int32), query_grid).reshape(
            token_count, head_cols
        )
        portion = jax.tree.map(
            lambda part: lax.all_gather(part, "tp", axis=1, tiled=True), shortened(attended)
        )
        out_rows = lax.slice_in_dim(w_out[layer_index], 0, portion.shape[1], axis=1)
        mixed = jnp.zeros((token_count, local_feats), jnp.float32) + contract(portion, out_rows)
        stream = (res_float + mixed).astype(jnp.bfloat16)
    return stream


def window_mask():
    shape = (GRID_W, 2 * GRID_W)
    key_col = lax.broadcasted_iota(jnp.int32, shape, 0)
    query_col = lax.broadcasted_iota(jnp.int32, shape, 1) % GRID_W
    first = jnp.clip(query_col - NA_COLS // 2, 0, GRID_W - NA_COLS)
    return (key_col >= first) & (key_col < first + NA_COLS)


def flip_matrix(count, base):
    shape = (count, 2 * GRID_W)
    source = lax.broadcasted_iota(jnp.int32, shape, 0)
    lane = lax.broadcasted_iota(jnp.int32, shape, 1)
    return (lane == base + count - 1 - source).astype(jnp.float32)


def pair_lanes(bias):
    row_offs, heads, col_offs = bias.shape
    flat = bias.reshape(row_offs * heads, col_offs)
    low, high = (
        jnp.dot(
            flat,
            flip_matrix(col_offs, base),
            precision=lax.Precision.HIGHEST,
            preferred_element_type=jnp.float32,
        )
        for base in (0, GRID_W)
    )
    return low, high


def build_table(lanes_of, table):
    inside = window_mask()
    for off in range(2 * NA_ROWS - 1):
        row = jnp.broadcast_to(lanes_of(off), (GRID_W, 2 * GRID_W))
        rolled = pltpu.roll(row, 2 * GRID_W - (NA_COLS - 1), axis=1, stride=1, stride_axis=0)
        table[off * GRID_W : (off + 1) * GRID_W, :] = jnp.where(inside, rolled, -1e30)


def attend_row(query, window_keys, window_values, bias):
    low = lax.broadcasted_iota(jnp.int32, query.shape, 1) < HEAD_DIM
    zero = jnp.zeros_like(query)
    block = jnp.concatenate([jnp.where(low, query, zero), jnp.where(low, zero, query)], axis=0)
    scores = contract(window_keys, block) + bias
    top = jnp.max(scores, axis=0, keepdims=True)
    weights = jnp.exp(scores - top)
    inverse = 1.0 / jnp.sum(weights, axis=0, keepdims=True)
    weights = (weights * inverse).astype(jnp.bfloat16)
    mixed = lax.dot_general(
        weights, window_values, (((0,), (0,)), ((), ())), preferred_element_type=jnp.float32
    )
    return jnp.where(low, mixed[:GRID_W], mixed[GRID_W:]).astype(jnp.bfloat16)


MESH = pl.DeviceIdType.MESH
REACH = NA_ROWS // 2
UP, DOWN = REACH, NA_ROWS - REACH - 1
AHEAD = 4
PERIOD = 16
FINISH, ATTEND, RELAY, LAST = 2, 6, 11, 13
TALL = 2 * GRID_W


def tp_copy(src, dst, sems, index, peer):
    return pltpu.make_async_remote_copy(
        src_ref=src,
        dst_ref=dst,
        send_sem=sems.at[0, index],
        recv_sem=sems.at[1, index],
        device_id=(lax.axis_index("sp"), peer),
        device_id_type=MESH,
    )


class SquareGather:
    def __init__(self, slots, sems, row_of):
        self.slots, self.sems, self.row_of = slots, sems, row_of
        self.me = lax.axis_index("tp")
        self.across = self.me + 1 - 2 * (self.me % 2)
        self.over = (self.me + 2) % 4
        self.corner = (self.across + 2) % 4

    def copy(self, kind, slot, index, peer):
        start, size = self.row_of(index) * GRID_W, GRID_W
        if kind >= 2:
            size = GRID_W // 2
            start = start + (kind - 2) * size
        part = self.slots.at[slot, pl.ds(pl.multiple_of(start, size), size), :]
        return tp_copy(part, part, self.sems.at[kind], index, peer)

    def send(self, index):
        self.copy(0, self.me, index, self.across).start()
        self.copy(1, self.me, index, self.over).start()

    def relay(self, index):
        self.copy(0, self.across, index, self.across).wait_recv()
        self.copy(2, self.across, index, self.over).start()
        self.copy(1, self.over, index, self.over).wait_recv()
        self.copy(3, self.over, index, self.across).start()

    def finish(self, index):
        self.copy(2, self.corner, index, self.over).wait_recv()
        self.copy(3, self.corner, index, self.across).wait_recv()

    def drain(self, index):
        self.copy(0, self.me, index, self.across).wait_send()
        self.copy(1, self.me, index, self.over).wait_send()
        self.copy(2, self.across, index, self.over).wait_send()
        self.copy(3, self.over, index, self.across).wait_send()


def halo_needs(rows_dev, sp_size):
    rows_all = rows_dev * sp_size
    picks = {"first": 0, "last": sp_size - 1}
    if sp_size > 2:
        picks.update(even=2, odd=1)
    needs = {}
    for kind, sp in picks.items():
        base, seen, steps = sp * rows_dev, set(), []
        for index in range(rows_dev):
            row = base + (rows_dev - 1 - index if sp % 2 else index)
            start = min(max(row - REACH, 0), rows_all - NA_ROWS)
            window = range(start, start + NA_ROWS)
            new = [(True, k) for k in range(UP) if base - UP + k in window]
            new += [(False, k) for k in range(DOWN) if base + rows_dev + k in window]
            steps.append([need for need in new if need not in seen])
            seen.update(new)
        for k in range(UP):
            if sp > 0 and (True, k) not in seen:
                steps[-1].append((True, k))
        for k in range(DOWN):
            if sp < sp_size - 1 and (False, k) not in seen:
                steps[-1].append((False, k))
        needs[kind] = steps
    return needs


def stack_kernel(
    rows_dev, needs,
    x_ref, gain_ref, bias_ref, wq_ref, wk_ref, wv_ref, wo_ref, out_ref,
    gains, weights, stream, mixed, keyval, queries, scaled, squares, sums, tables, bias, partial,
    weight_sems, gain_sems, stream_sems, mixed_sems, halo_sems, local_sems,
):
    sp, sp_size = lax.axis_index("sp"), lax.axis_size("sp")
    layers = wq_ref.shape[0]
    tokens, feats = x_ref.shape
    width, total_feats = feats, 4 * feats
    odd = sp % 2

    def row_of(index):
        return index + odd * (rows_dev - 1 - 2 * index)

    streams = SquareGather(stream, stream_sems, row_of)
    mixes = SquareGather(mixed, mixed_sems, row_of)
    me, across, over, corner = streams.me, streams.across, streams.over, streams.corner
    sources = (wk_ref, wv_ref, wq_ref, wo_ref)

    def rows_at(row):
        return pl.ds(pl.multiple_of(row * GRID_W, GRID_W), GRID_W)

    def pair_at(index):
        low = jnp.minimum(row_of(index), row_of(index - 1))
        return pl.ds(pl.multiple_of(low * GRID_W, TALL), TALL)

    def weight_copy(kind, layer):
        return pltpu.make_async_copy(
            sources[kind].at[layer], weights.at[kind, layer], weight_sems.at[kind, layer]
        )

    load_x = pltpu.make_async_copy(x_ref, stream.at[me], local_sems.at[rows_dev])
    load_bias = pltpu.make_async_copy(bias_ref, bias, local_sems.at[rows_dev + 1])
    load_x.start()
    load_bias.start()

    barrier = pltpu.get_barrier_semaphore()
    for peer in (across, over, corner):
        pl.semaphore_signal(barrier, inc=1, device_id=(sp, peer), device_id_type=MESH)

    @pl.when(sp > 0)
    def _():
        pl.semaphore_signal(barrier, inc=1, device_id=(sp - 1, me), device_id_type=MESH)

    @pl.when(sp < sp_size - 1)
    def _():
        pl.semaphore_signal(barrier, inc=1, device_id=(sp + 1, me), device_id_type=MESH)

    for layer in range(layers):
        for kind in range(4):
            weight_copy(kind, layer).start()

    gains[me, 0:layers, :] = gain_ref[...].astype(jnp.float32)
    sides = jnp.minimum(sp, 1) + jnp.minimum(sp_size - 1 - sp, 1)
    load_x.wait()
    pl.semaphore_wait(barrier, 3 + sides)

    def gain_copy(index, slot, peer):
        return tp_copy(gains.at[slot], gains.at[slot], gain_sems, index, peer)

    for index, peer in enumerate((across, over, corner)):
        gain_copy(index, me, peer).start()
    for index in range(AHEAD):
        streams.send(index)

    def halo_copy(parity, up, k):
        local = rows_dev - UP + k if up else k
        there = k if up else UP + rows_dev + k
        return pltpu.make_async_remote_copy(
            src_ref=keyval.at[parity, rows_at(UP + local), :],
            dst_ref=keyval.at[parity, rows_at(there), :],
            send_sem=halo_sems.at[0, parity, int(up), k],
            recv_sem=halo_sems.at[1, parity, int(up), k],
            device_id=(sp + 1 if up else sp - 1, me),
            device_id_type=MESH,
        )

    def project(layer, slot, kind, source):
        cols = pl.ds(pl.multiple_of(slot * width, width), width)
        return contract(source, weights[kind, layer, :, cols])

    def scale_slot(layer, slot, here):
        part = stream[slot, here, :].astype(jnp.float32)
        square = part * part
        folded = square[:, :128]
        for start in range(128, feats, 128):
            folded += square[:, start : start + 128]
        return (part * gains[slot, pl.ds(layer, 1), :]).astype(jnp.bfloat16), folded

    def drain_mixed(index):
        for row in range(AHEAD - 1, rows_dev):

            @pl.when(index == row)
            def _(row=row):
                last = rows_dev if row == rows_dev - 1 else row - DOWN + 1
                for done in range(row - DOWN, last):
                    mixes.drain(done)

    def relay_stream(layer, index):
        @pl.when((layer == 0) & (index == 0))
        def _():
            load_bias.wait()
            for place, peer in enumerate((across, over, corner)):
                gain_copy(place, peer, peer).wait_recv()
                gain_copy(place, me, peer).wait_send()

        streams.relay(index)

        @pl.when((layer == 0) & (index + AHEAD < rows_dev))
        def _():
            streams.send(index + AHEAD)

        @pl.when(index == 0)
        def _():
            for kind in range(3):
                weight_copy(kind, layer).wait()

    def start_pair(layer, index):
        here, turn = pair_at(index), index // 2 % 2
        folded = jnp.zeros((TALL, 128), jnp.float32)
        for place, slot in enumerate((me, across, over)):
            scaled[place], square = scale_slot(layer, slot, here)
            folded += square
        squares[turn] = folded
        for kind in range(3):
            total = project(layer, me, kind, scaled[0])
            total += project(layer, across, kind, scaled[1])
            sums[turn, kind] = total + project(layer, over, kind, scaled[2])

    def end_pair(layer, index):
        here, turn, parity = pair_at(index), index // 2 % 2, layer % 2
        streams.finish(index - 1)
        streams.finish(index)
        source, folded = scale_slot(layer, corner, here)
        total = jnp.sum(squares[turn] + folded, axis=1, keepdims=True)
        inverse = lax.rsqrt(total * (1.0 / total_feats) + epsilon)
        there = pl.ds(pl.multiple_of(here.start + UP * GRID_W, GRID_W), TALL)
        for kind in range(2):
            keyval[parity, there, kind * width : (kind + 1) * width] = (
                (sums[turn, kind] + project(layer, corner, kind, source)) * inverse
            ).astype(jnp.bfloat16)
        for row in (row_of(index - 1), row_of(index)):

            @pl.when((row < DOWN) & (sp > 0))
            def _(row=row):
                halo_copy(parity, False, row).start()

            @pl.when((row >= rows_dev - UP) & (sp < sp_size - 1))
            def _(row=row):
                halo_copy(parity, True, row - (rows_dev - UP)).start()

        queries[here, :] = (
            (sums[turn, 2] + project(layer, corner, 2, source)) * inverse
        ).astype(jnp.bfloat16) * jnp.bfloat16(HEAD_DIM ** (-0.5))

    def make_tables(layer, index):
        @pl.when(index == 0)
        def _():
            low, high = pair_lanes(bias[layer])
            heads = bias.shape[2]

            def lanes_of(pair):
                def at(off):
                    place = off * heads + 2 * pair
                    return low[place : place + 1] + high[place + 1 : place + 2]

                return at

            for pair in range(width // 128):
                build_table(lanes_of(pair), tables.at[pair])

    kinds = {
        "first": sp == 0,
        "last": sp == sp_size - 1,
        "even": (odd == 0) & (sp > 0),
        "odd": (odd == 1) & (sp < sp_size - 1),
    }

    def wait_halo(parity, index):
        for kind, steps in needs.items():
            for step, rows in enumerate(steps):
                if rows:

                    @pl.when(kinds[kind] & (index == step))
                    def _(rows=rows):
                        for up, k in rows:
                            halo_copy(parity, up, k).wait_recv()

    def attend(layer, index):
        row, parity = row_of(index), layer % 2
        here = rows_at(row)
        wait_halo(parity, index)
        base = sp * rows_dev
        first = jnp.clip(base + row - REACH, 0, rows_dev * sp_size - NA_ROWS)
        start, off = first - base + UP, first - base - row + NA_ROWS - 1
        keys = pl.ds(pl.multiple_of(start * GRID_W, GRID_W), NA_ROWS * GRID_W)
        offs = pl.ds(pl.multiple_of(off * GRID_W, GRID_W), NA_ROWS * GRID_W)
        for pair in range(width // 128):
            cols = slice(pair * 128, (pair + 1) * 128)
            vcols = slice(width + pair * 128, width + (pair + 1) * 128)
            mixed[me, here, cols] = attend_row(
                queries[here, cols],
                keyval[parity, keys, cols],
                keyval[parity, keys, vcols],
                tables[pair, offs, :],
            )
        streams.drain(index)
        mixes.send(index)

        @pl.when(index == rows_dev - 1)
        def _():
            @pl.when(sp > 0)
            def _():
                for k in range(DOWN):
                    halo_copy(parity, False, k).wait_send()

            @pl.when(sp < sp_size - 1)
            def _():
                for k in range(UP):
                    halo_copy(parity, True, k).wait_send()

    def relay_mixed(layer, index):
        mixes.relay(index)

        @pl.when(index == 0)
        def _():
            weight_copy(3, layer).wait()

    def start_mixed(layer, index):
        here = pair_at(index)
        total = stream[me, here, :].astype(jnp.float32)
        for slot in (me, across, over):
            total += project(layer, slot, 3, mixed[slot, here, :])
        partial[index // 2 % 2] = total

    def store_out(index):
        here = pair_at(index)
        return pltpu.make_async_copy(
            stream.at[me, here, :], out_ref.at[here, :], local_sems.at[index]
        )

    def end_mixed(layer, index):
        here = pair_at(index)
        mixes.finish(index - 1)
        mixes.finish(index)
        total = partial[index // 2 % 2] + project(layer, corner, 3, mixed[corner, here, :])
        stream[me, here, :] = total.astype(jnp.bfloat16)

        @pl.when(layer < layers - 1)
        def _():
            for row in (index - 1, index):
                drain_mixed(row)
                streams.send(row)

        @pl.when(layer == layers - 1)
        def _():
            store_out(index).start()

    early = (odd == 0) & (sp > 0)
    steps = (
        (relay_mixed, RELAY, 1),
        (start_mixed, RELAY, 2),
        (end_mixed, LAST, 2),
        (relay_stream, 0, 1),
        (end_pair, FINISH, 2),
        (start_pair, 0, 2),
        (make_tables, 0, 1),
        (attend, ATTEND + 1 - early.astype(jnp.int32), 1),
    )

    def tick(now, carry):
        for step, delay, rows in steps:
            since = now - delay

            @pl.when((since >= 0) & (since < layers * PERIOD))
            def _(step=step, since=since, rows=rows):
                layer, index = since // PERIOD, since % PERIOD

                @pl.when((index < rows_dev) & (index % rows == rows - 1))
                def _():
                    step(layer, index)

        return carry

    lax.fori_loop(0, PERIOD * (layers - 1) + LAST + rows_dev, tick, 0)
    for index in range(rows_dev):
        mixes.drain(index)
    for index in range(1, rows_dev, 2):
        store_out(index).wait()


def square_device(residual, norm_gain, w_query, w_key, w_value, w_out, offset_bias):
    tokens, feats = residual.shape
    layers, heads, row_offs, col_offs = offset_bias.shape
    rows_dev = tokens // GRID_W
    vmem = pl.BlockSpec(memory_space=pltpu.VMEM)
    hbm = pl.BlockSpec(memory_space=pl.ANY)
    bf16, f32, dma = jnp.bfloat16, jnp.float32, pltpu.SemaphoreType.DMA
    padded = tokens + (UP + DOWN) * GRID_W
    needs = halo_needs(rows_dev, lax.axis_size("sp"))
    return pl.pallas_call(
        lambda *refs: stack_kernel(rows_dev, needs, *refs),
        out_shape=jax.ShapeDtypeStruct(residual.shape, bf16),
        in_specs=[hbm, vmem] + [hbm] * 5,
        out_specs=hbm,
        scratch_shapes=[
            pltpu.VMEM((4, -(-layers // 8) * 8, feats), f32),
            pltpu.VMEM((4,) + w_query.shape, bf16),
            pltpu.VMEM((4, tokens, feats), bf16),
            pltpu.VMEM((4, tokens, feats), bf16),
            pltpu.VMEM((2, padded, 2 * feats), bf16),
            pltpu.VMEM((tokens, feats), bf16),
            pltpu.VMEM((3, TALL, feats), bf16),
            pltpu.VMEM((2, TALL, 128), f32),
            pltpu.VMEM((2, 3, TALL, feats), f32),
            pltpu.VMEM((feats // 128, row_offs * GRID_W, 128), f32),
            pltpu.VMEM((layers, row_offs, heads, col_offs), f32),
            pltpu.VMEM((2, TALL, feats), f32),
            dma((4, layers)),
            dma((2, 3)),
            dma((4, 2, rows_dev)),
            dma((4, 2, rows_dev)),
            dma((2, 2, 2, max(UP, DOWN))),
            dma((rows_dev + 2,)),
        ],
        compiler_params=pltpu.CompilerParams(
            collective_id=0, has_side_effects=True, vmem_limit_bytes=56 * 1024 * 1024
        ),
        name="stack",
    )(residual, norm_gain, offset_bias.transpose(0, 2, 1, 3), w_query, w_key, w_value, w_out)


def per_device(residual, norm_gain, w_query, w_key, w_value, w_out, offset_bias):
    paired = offset_bias.shape[1] % 8 == 0 and 2 * HEAD_DIM == 128 and 2 * GRID_W == 128
    square = lax.axis_size("tp") == 4 and offset_bias.shape[1] * HEAD_DIM == residual.shape[1]
    rows_dev = residual.shape[0] // GRID_W
    even = lax.axis_size("sp") % 2 == 0 and rows_dev == ATTEND
    body = generic_device
    if paired and square and even:
        body = square_device
    return body(residual, norm_gain, w_query, w_key, w_value, w_out, offset_bias)


def solution(mesh):
    in_specs = (
        P("sp", "tp"),
        P(None, "tp"),
        P(None, "tp", None),
        P(None, "tp", None),
        P(None, "tp", None),
        P(None, "tp", None),
        P(None, "tp", None, None),
    )
    out_specs = P("sp", "tp")
    return jax.shard_map(
        per_device, mesh=mesh, in_specs=in_specs, out_specs=out_specs, check_vma=False
    )
```

time: 118 us -> 109 us (0.924)
  Pallas kernels: 113 us -> 106 us
  local copies, waits for them, and re-layouts: 3.69 us -> 1.77 us
    pallas_call x1, Pallas kernels: 113 us -> 106 us  [square_device(): pl.pallas_call(lambda *refs: stack_kernel(rows_dev, needs, *refs), out_sh...]
where the time goes in v1:
time: 109 us; the launch traced here: 108 us
  Pallas kernels  106 us (97%)
  local copies, waits for them, and re-layouts  1.77 us (2%)
    pallas_call x1, Pallas kernels, square_device(): pl.pallas_call(lambda *refs: stack_kernel(rows_dev, needs, *refs), out_sh...  106 us

profile of v1, /device:TPU:8, one launch (start us, length us, event | category | flops | bytes accessed | tf_op | source)
XLA Modules:
  0.0 107.5 jit_solution(4900301568786243602)
XLA Ops:
  0.0 105.7 %stack.1 = bf16[384,512]{1,0:T(8,128)(2,1)} custom-call(bf16[384,512]{1,0:T(8,128)(2,1)} %refs_0_.1, bf16[3,512]{1,0:T(4,128)(2,1)} %refs_1_.1, f32[3,15,8,31]{3,2,1,0:T(8,128)} %bitcast.1, bf16[3,512,2048]{2,1,0:T(8,128)(2,1)} %refs_3_.1, bf16[3,512,2048]{2,1,0:T(8,128)(2,1)} %refs_4_.1, bf16[3,512,2048]{2,1,0:T(8,128)(2,1)} %refs_5_.1, ...), custom_call_target="tpu_custom_call" | custom-call | tf_op jit(solution)/shard_map/stack/pallas_call | solution.py:574
  105.7 1.8 %copy.9 = bf16[384,512]{1,0:T(8,128)(2,1)} copy(bf16[384,512]{1,0:T(8,128)(2,1)} %stack.1) | data formatting | bytes 786432

commit v2 on v1

--- a/solution.py
+++ b/solution.py
@@ -169,7 +169,7 @@
     for off in range(2 * NA_ROWS - 1):
         row = jnp.broadcast_to(lanes_of(off), (GRID_W, 2 * GRID_W))
         rolled = pltpu.roll(row, 2 * GRID_W - (NA_COLS - 1), axis=1, stride=1, stride_axis=0)
-        table[off * GRID_W : (off + 1) * GRID_W, :] = jnp.where(inside, rolled, -1e30)
+        table[off * GRID_W : (off + 1) * GRID_W, :] = jnp.where(inside, rolled * LOG2E, -1e30)
 
 
 def attend_row(query, window_keys, window_values, bias):
@@ -177,22 +177,21 @@
     zero = jnp.zeros_like(query)
     block = jnp.concatenate([jnp.where(low, query, zero), jnp.where(low, zero, query)], axis=0)
     scores = contract(window_keys, block) + bias
-    top = jnp.max(scores, axis=0, keepdims=True)
-    weights = jnp.exp(scores - top)
-    inverse = 1.0 / jnp.sum(weights, axis=0, keepdims=True)
-    weights = (weights * inverse).astype(jnp.bfloat16)
+    weights = jnp.exp2(scores - jnp.max(scores, axis=0, keepdims=True)).astype(jnp.bfloat16)
+    ones = jnp.ones_like(window_values)
     mixed = lax.dot_general(
-        weights, window_values, (((0,), (0,)), ((), ())), preferred_element_type=jnp.float32
+        weights, jnp.concatenate([window_values, ones], axis=1), (((0,), (0,)), ((), ())),
+        preferred_element_type=jnp.float32,
     )
+    mixed = mixed[:, : 2 * HEAD_DIM] / mixed[:, 2 * HEAD_DIM :]
     return jnp.where(low, mixed[:GRID_W], mixed[GRID_W:]).astype(jnp.bfloat16)
 
 
 MESH = pl.DeviceIdType.MESH
+LOG2E = 1.4426950408889634
 REACH = NA_ROWS // 2
 UP, DOWN = REACH, NA_ROWS - REACH - 1
 AHEAD = 4
-PERIOD = 16
-FINISH, ATTEND, RELAY, LAST = 2, 6, 11, 13
 TALL = 2 * GRID_W
 
 
@@ -208,40 +207,49 @@
 
 
 class SquareGather:
-    def __init__(self, slots, sems, row_of):
-        self.slots, self.sems, self.row_of = slots, sems, row_of
+    def __init__(self, slots, sems, row_of, halves):
+        self.slots, self.sems, self.row_of, self.halves = slots, sems, row_of, halves
         self.me = lax.axis_index("tp")
         self.across = self.me + 1 - 2 * (self.me % 2)
         self.over = (self.me + 2) % 4
         self.corner = (self.across + 2) % 4
 
-    def copy(self, kind, slot, index, peer):
-        start, size = self.row_of(index) * GRID_W, GRID_W
-        if kind >= 2:
-            size = GRID_W // 2
-            start = start + (kind - 2) * size
-        part = self.slots.at[slot, pl.ds(pl.multiple_of(start, size), size), :]
-        return tp_copy(part, part, self.sems.at[kind], index, peer)
-
-    def send(self, index):
-        self.copy(0, self.me, index, self.across).start()
-        self.copy(1, self.me, index, self.over).start()
-
-    def relay(self, index):
-        self.copy(0, self.across, index, self.across).wait_recv()
-        self.copy(2, self.across, index, self.over).start()
-        self.copy(1, self.over, index, self.over).wait_recv()
-        self.copy(3, self.over, index, self.across).start()
+    def copy(self, kind, slot, index, half, peer):
+        start = pl.multiple_of(self.row_of(index) * GRID_W, GRID_W)
+        width = self.slots.shape[2]
+        if kind == 2 or self.halves == 2:
+            width = width // 2
+        cols = slice(half * width, (half + 1) * width)
+        part = self.slots.at[slot, pl.ds(start, GRID_W), cols]
+        return tp_copy(part, part, self.sems.at[kind], 2 * index + half, peer)
+
+    def send(self, index, half=0):
+        self.copy(0, self.me, index, half, self.across).start()
+        self.copy(1, self.me, index, half, self.over).start()
+
+    def relay(self, index, half):
+        take = half if self.halves == 2 else 0
+        if half == 0:
+            self.copy(0, self.across, index, take, self.across).wait_recv()
+            self.copy(2, self.across, index, half, self.over).start()
+        else:
+            self.copy(1, self.over, index, take, self.over).wait_recv()
+            self.copy(2, self.over, index, half, self.across).start()
+
+    def settle(self, index):
+        self.copy(0, self.across, index, 1, self.across).wait_recv()
+        self.copy(1, self.over, index, 0, self.over).wait_recv()
 
     def finish(self, index):
-        self.copy(2, self.corner, index, self.over).wait_recv()
-        self.copy(3, self.corner, index, self.across).wait_recv()
+        self.copy(2, self.corner, index, 0, self.over).wait_recv()
+        self.copy(2, self.corner, index, 1, self.across).wait_recv()
 
     def drain(self, index):
-        self.copy(0, self.me, index, self.across).wait_send()
-        self.copy(1, self.me, index, self.over).wait_send()
-        self.copy(2, self.across, index, self.over).wait_send()
-        self.copy(3, self.over, index, self.across).wait_send()
+        for half in range(self.halves):
+            self.copy(0, self.me, index, half, self.across).wait_send()
+            self.copy(1, self.me, index, half, self.over).wait_send()
+        self.copy(2, self.across, index, 0, self.over).wait_send()
+        self.copy(2, self.over, index, 1, self.across).wait_send()
 
 
 def halo_needs(rows_dev, sp_size):
@@ -253,7 +261,7 @@
     for kind, sp in picks.items():
         base, seen, steps = sp * rows_dev, set(), []
         for index in range(rows_dev):
-            row = base + (rows_dev - 1 - index if sp % 2 else index)
+            row = base + (index if sp % 2 else rows_dev - 1 - index)
             start = min(max(row - REACH, 0), rows_all - NA_ROWS)
             window = range(start, start + NA_ROWS)
             new = [(True, k) for k in range(UP) if base - UP + k in window]
@@ -280,21 +288,21 @@
     layers = wq_ref.shape[0]
     tokens, feats = x_ref.shape
     width, total_feats = feats, 4 * feats
-    odd = sp % 2
+    even = 1 - sp % 2
 
     def row_of(index):
-        return index + odd * (rows_dev - 1 - 2 * index)
-
-    streams = SquareGather(stream, stream_sems, row_of)
-    mixes = SquareGather(mixed, mixed_sems, row_of)
+        return index + even * (rows_dev - 1 - 2 * index)
+
+    streams = SquareGather(stream, stream_sems, row_of, 1)
+    mixes = SquareGather(mixed, mixed_sems, row_of, 2)
     me, across, over, corner = streams.me, streams.across, streams.over, streams.corner
     sources = (wk_ref, wv_ref, wq_ref, wo_ref)
 
     def rows_at(row):
         return pl.ds(pl.multiple_of(row * GRID_W, GRID_W), GRID_W)
 
-    def pair_at(index):
-        low = jnp.minimum(row_of(index), row_of(index - 1))
+    def pair_at(chunk):
+        low = jnp.minimum(row_of(2 * chunk), row_of(2 * chunk + 1))
         return pl.ds(pl.multiple_of(low * GRID_W, TALL), TALL)
 
     def weight_copy(kind, layer):
@@ -360,59 +368,67 @@
             folded += square[:, start : start + 128]
         return (part * gains[slot, pl.ds(layer, 1), :]).astype(jnp.bfloat16), folded
 
-    def drain_mixed(index):
-        for row in range(AHEAD - 1, rows_dev):
-
-            @pl.when(index == row)
-            def _(row=row):
-                last = rows_dev if row == rows_dev - 1 else row - DOWN + 1
-                for done in range(row - DOWN, last):
-                    mixes.drain(done)
+    def drain_mixed(row):
+        if row >= DOWN:
+            last = rows_dev if row == rows_dev - 1 else row - DOWN + 1
+            for done in range(row - DOWN, last):
+                mixes.drain(done)
 
     def relay_stream(layer, index):
-        @pl.when((layer == 0) & (index == 0))
-        def _():
-            load_bias.wait()
-            for place, peer in enumerate((across, over, corner)):
-                gain_copy(place, peer, peer).wait_recv()
-                gain_copy(place, me, peer).wait_send()
-
-        streams.relay(index)
-
-        @pl.when((layer == 0) & (index + AHEAD < rows_dev))
-        def _():
-            streams.send(index + AHEAD)
-
-        @pl.when(index == 0)
-        def _():
-            for kind in range(3):
-                weight_copy(kind, layer).wait()
-
-    def start_pair(layer, index):
-        here, turn = pair_at(index), index // 2 % 2
-        folded = jnp.zeros((TALL, 128), jnp.float32)
-        for place, slot in enumerate((me, across, over)):
-            scaled[place], square = scale_slot(layer, slot, here)
-            folded += square
-        squares[turn] = folded
-        for kind in range(3):
-            total = project(layer, me, kind, scaled[0])
-            total += project(layer, across, kind, scaled[1])
-            sums[turn, kind] = total + project(layer, over, kind, scaled[2])
-
-    def end_pair(layer, index):
-        here, turn, parity = pair_at(index), index // 2 % 2, layer % 2
-        streams.finish(index - 1)
-        streams.finish(index)
+        if index == 0:
+
+            @pl.when(layer == 0)
+            def _():
+                for place, peer in enumerate((across, over, corner)):
+                    gain_copy(place, peer, peer).wait_recv()
+                    gain_copy(place, me, peer).wait_send()
+
+        streams.relay(index, 0)
+        streams.relay(index, 1)
+        if index + AHEAD < rows_dev:
+
+            @pl.when(layer == 0)
+            def _():
+                streams.send(index + AHEAD)
+
+    def start_rows(layer, chunk, kind):
+        here = pair_at(chunk)
+        slots = (me, across, over)
+        if kind == 0:
+            folded = jnp.zeros((TALL, 128), jnp.float32)
+            for place, slot in enumerate(slots):
+                scaled[chunk, place], square = scale_slot(layer, slot, here)
+                folded += square
+            squares[chunk] = folded
+        if chunk == 0:
+            weight_copy(kind, layer).wait()
+        sums[chunk, kind] = sum(
+            project(layer, slot, kind, scaled[chunk, place]) for place, slot in enumerate(slots)
+        )
+
+    def end_rows(layer, chunk, part):
+        here, parity = pair_at(chunk), layer % 2
+        if part == 1:
+            queries[here, :] = (
+                (sums[chunk, 2] + project(layer, corner, 2, scaled[chunk, 3]))
+                * (squares[chunk, :, :1] * (HEAD_DIM ** (-0.5) * LOG2E))
+            ).astype(jnp.bfloat16)
+            return
+        rows = (2 * chunk, 2 * chunk + 1)
+        for index in rows:
+            streams.finish(index)
         source, folded = scale_slot(layer, corner, here)
-        total = jnp.sum(squares[turn] + folded, axis=1, keepdims=True)
+        scaled[chunk, 3] = source
+        total = jnp.sum(squares[chunk] + folded, axis=1, keepdims=True)
         inverse = lax.rsqrt(total * (1.0 / total_feats) + epsilon)
+        squares[chunk] = jnp.broadcast_to(inverse, (TALL, 128))
         there = pl.ds(pl.multiple_of(here.start + UP * GRID_W, GRID_W), TALL)
         for kind in range(2):
             keyval[parity, there, kind * width : (kind + 1) * width] = (
-                (sums[turn, kind] + project(layer, corner, kind, source)) * inverse
+                (sums[chunk, kind] + project(layer, corner, kind, source)) * inverse
             ).astype(jnp.bfloat16)
-        for row in (row_of(index - 1), row_of(index)):
+        for index in rows:
+            row = row_of(index)
 
             @pl.when((row < DOWN) & (sp > 0))
             def _(row=row):
@@ -422,53 +438,53 @@
             def _(row=row):
                 halo_copy(parity, True, row - (rows_dev - UP)).start()
 
-        queries[here, :] = (
-            (sums[turn, 2] + project(layer, corner, 2, source)) * inverse
-        ).astype(jnp.bfloat16) * jnp.bfloat16(HEAD_DIM ** (-0.5))
-
-    def make_tables(layer, index):
-        @pl.when(index == 0)
+    def make_tables(layer):
+        @pl.when(layer == 0)
         def _():
-            low, high = pair_lanes(bias[layer])
-            heads = bias.shape[2]
-
-            def lanes_of(pair):
-                def at(off):
-                    place = off * heads + 2 * pair
-                    return low[place : place + 1] + high[place + 1 : place + 2]
-
-                return at
-
-            for pair in range(width // 128):
-                build_table(lanes_of(pair), tables.at[pair])
+            load_bias.wait()
+
+        low, high = pair_lanes(bias[layer])
+        heads = bias.shape[2]
+
+        def lanes_of(pair):
+            def at(off):
+                place = off * heads + 2 * pair
+                return low[place : place + 1] + high[place + 1 : place + 2]
+
+            return at
+
+        for pair in range(width // 128):
+            build_table(lanes_of(pair), tables.at[pair])
 
     kinds = {
         "first": sp == 0,
         "last": sp == sp_size - 1,
-        "even": (odd == 0) & (sp > 0),
-        "odd": (odd == 1) & (sp < sp_size - 1),
+        "even": (even == 1) & (sp > 0),
+        "odd": (even == 0) & (sp < sp_size - 1),
     }
+    early = kinds["odd"]
 
     def wait_halo(parity, index):
         for kind, steps in needs.items():
-            for step, rows in enumerate(steps):
-                if rows:
-
-                    @pl.when(kinds[kind] & (index == step))
-                    def _(rows=rows):
-                        for up, k in rows:
-                            halo_copy(parity, up, k).wait_recv()
-
-    def attend(layer, index):
+            if steps[index]:
+
+                @pl.when(kinds[kind])
+                def _(rows=steps[index]):
+                    for up, k in rows:
+                        halo_copy(parity, up, k).wait_recv()
+
+    def attend(layer, index, half):
         row, parity = row_of(index), layer % 2
         here = rows_at(row)
-        wait_halo(parity, index)
+        if half == 0:
+            wait_halo(parity, index)
         base = sp * rows_dev
         first = jnp.clip(base + row - REACH, 0, rows_dev * sp_size - NA_ROWS)
         start, off = first - base + UP, first - base - row + NA_ROWS - 1
         keys = pl.ds(pl.multiple_of(start * GRID_W, GRID_W), NA_ROWS * GRID_W)
         offs = pl.ds(pl.multiple_of(off * GRID_W, GRID_W), NA_ROWS * GRID_W)
-        for pair in range(width // 128):
+        pairs = width // 256
+        for pair in range(half * pairs, (half + 1) * pairs):
             cols = slice(pair * 128, (pair + 1) * 128)
             vcols = slice(width + pair * 128, width + (pair + 1) * 128)
             mixed[me, here, cols] = attend_row(
@@ -477,11 +493,11 @@
                 keyval[parity, keys, vcols],
                 tables[pair, offs, :],
             )
-        streams.drain(index)
-        mixes.send(index)
-
-        @pl.when(index == rows_dev - 1)
-        def _():
+        if half == 1:
+            streams.drain(index)
+        mixes.send(index, half)
+        if index == rows_dev - 1 and half == 1:
+
             @pl.when(sp > 0)
             def _():
                 for k in range(DOWN):
@@ -492,74 +508,120 @@
                 for k in range(UP):
                     halo_copy(parity, True, k).wait_send()
 
-    def relay_mixed(layer, index):
-        mixes.relay(index)
-
-        @pl.when(index == 0)
-        def _():
+    def relay_mixed(layer, index, half):
+        mixes.relay(index, half)
+
+    def start_mixed(layer, chunk):
+        here = pair_at(chunk)
+        for index in (2 * chunk, 2 * chunk + 1):
+            mixes.settle(index)
+        if chunk == 0:
             weight_copy(3, layer).wait()
-
-    def start_mixed(layer, index):
-        here = pair_at(index)
         total = stream[me, here, :].astype(jnp.float32)
         for slot in (me, across, over):
             total += project(layer, slot, 3, mixed[slot, here, :])
-        partial[index // 2 % 2] = total
-
-    def store_out(index):
-        here = pair_at(index)
+        partial[chunk] = total
+
+    def store_out(chunk):
+        here = pair_at(chunk)
         return pltpu.make_async_copy(
-            stream.at[me, here, :], out_ref.at[here, :], local_sems.at[index]
-        )
-
-    def end_mixed(layer, index):
-        here = pair_at(index)
-        mixes.finish(index - 1)
-        mixes.finish(index)
-        total = partial[index // 2 % 2] + project(layer, corner, 3, mixed[corner, here, :])
+            stream.at[me, here, :], out_ref.at[here, :], local_sems.at[chunk]
+        )
+
+    def end_mixed(layer, chunk):
+        here = pair_at(chunk)
+        rows = (2 * chunk, 2 * chunk + 1)
+        for index in rows:
+            mixes.finish(index)
+        total = partial[chunk] + project(layer, corner, 3, mixed[corner, here, :])
         stream[me, here, :] = total.astype(jnp.bfloat16)
 
         @pl.when(layer < layers - 1)
         def _():
-            for row in (index - 1, index):
-                drain_mixed(row)
-                streams.send(row)
+            for index in rows:
+                drain_mixed(index)
+                streams.send(index)
 
         @pl.when(layer == layers - 1)
         def _():
-            store_out(index).start()
-
-    early = (odd == 0) & (sp > 0)
-    steps = (
-        (relay_mixed, RELAY, 1),
-        (start_mixed, RELAY, 2),
-        (end_mixed, LAST, 2),
-        (relay_stream, 0, 1),
-        (end_pair, FINISH, 2),
-        (start_pair, 0, 2),
-        (make_tables, 0, 1),
-        (attend, ATTEND + 1 - early.astype(jnp.int32), 1),
+            store_out(chunk).start()
+
+    plan = (
+        (make_tables, None),
+        (relay_stream, None, 0),
+        (relay_stream, None, 1),
+        (start_rows, None, 0, 0),
+        (start_rows, None, 0, 1),
+        (start_rows, None, 0, 2),
+        (relay_stream, None, 2),
+        (relay_stream, None, 3),
+        (start_rows, None, 1, 0),
+        (start_rows, None, 1, 1),
+        (start_rows, None, 1, 2),
+        (end_rows, None, 0, 0),
+        (relay_stream, None, 4),
+        (end_rows, None, 0, 1),
+        (end_rows, None, 1, 0),
+        (relay_stream, None, 5),
+        (start_rows, None, 2, 0),
+        (start_rows, None, 2, 1),
+        (start_rows, None, 2, 2),
+        (end_rows, None, 1, 1),
+        (end_rows, None, 2, 0),
+        (attend, early, 0, 0),
+        (attend, early, 0, 1),
+        (end_rows, None, 2, 1),
+        (attend, ~early, 0, 0),
+        (attend, ~early, 0, 1),
+        (attend, None, 1, 0),
+        (attend, None, 1, 1),
+        (attend, None, 2, 0),
+        (attend, None, 2, 1),
+        (attend, ~early, 3, 0),
+        (attend, ~early, 3, 1),
+        (attend, ~early, 4, 0),
+        (attend, ~early, 4, 1),
+        (attend, ~early, 5, 0),
+        (attend, ~early, 5, 1),
+        (relay_mixed, None, 0, 0),
+        (relay_mixed, None, 0, 1),
+        (relay_mixed, None, 1, 0),
+        (relay_mixed, None, 1, 1),
+        (relay_mixed, None, 2, 0),
+        (attend, early, 3, 0),
+        (attend, early, 3, 1),
+        (attend, early, 4, 0),
+        (attend, early, 4, 1),
+        (attend, early, 5, 0),
+        (attend, early, 5, 1),
+        (start_mixed, None, 0),
+        (relay_mixed, None, 2, 1),
+        (relay_mixed, None, 3, 0),
+        (relay_mixed, None, 3, 1),
+        (start_mixed, None, 1),
+        (relay_mixed, None, 4, 0),
+        (relay_mixed, None, 4, 1),
+        (relay_mixed, None, 5, 0),
+        (relay_mixed, None, 5, 1),
+        (end_mixed, None, 0),
+        (start_mixed, None, 2),
+        (end_mixed, None, 1),
+        (end_mixed, None, 2),
     )
 
-    def tick(now, carry):
-        for step, delay, rows in steps:
-            since = now - delay
-
-            @pl.when((since >= 0) & (since < layers * PERIOD))
-            def _(step=step, since=since, rows=rows):
-                layer, index = since // PERIOD, since % PERIOD
-
-                @pl.when((index < rows_dev) & (index % rows == rows - 1))
-                def _():
-                    step(layer, index)
-
+    def one_layer(layer, carry):
+        for step, when, *place in plan:
+            if when is None:
+                step(layer, *place)
+            else:
+                pl.when(when)(lambda: step(layer, *place))
         return carry
 
-    lax.fori_loop(0, PERIOD * (layers - 1) + LAST + rows_dev, tick, 0)
+    lax.fori_loop(0, layers, one_layer, 0)
     for index in range(rows_dev):
         mixes.drain(index)
-    for index in range(1, rows_dev, 2):
-        store_out(index).wait()
+    for chunk in range(rows_dev // 2):
+        store_out(chunk).wait()
 
 
 def square_device(residual, norm_gain, w_query, w_key, w_value, w_out, offset_bias):
@@ -583,16 +645,16 @@
             pltpu.VMEM((4, tokens, feats), bf16),
             pltpu.VMEM((2, padded, 2 * feats), bf16),
             pltpu.VMEM((tokens, feats), bf16),
-            pltpu.VMEM((3, TALL, feats), bf16),
-            pltpu.VMEM((2, TALL, 128), f32),
-            pltpu.VMEM((2, 3, TALL, feats), f32),
+            pltpu.VMEM((rows_dev // 2, 4, TALL, feats), bf16),
+            pltpu.VMEM((rows_dev // 2, TALL, 128), f32),
+            pltpu.VMEM((rows_dev // 2, 3, TALL, feats), f32),
             pltpu.VMEM((feats // 128, row_offs * GRID_W, 128), f32),
             pltpu.VMEM((layers, row_offs, heads, col_offs), f32),
-            pltpu.VMEM((2, TALL, feats), f32),
+            pltpu.VMEM((rows_dev // 2, TALL, feats), f32),
             dma((4, layers)),
             dma((2, 3)),
-            dma((4, 2, rows_dev)),
-            dma((4, 2, rows_dev)),
+            dma((3, 2, 2 * rows_dev)),
+            dma((3, 2, 2 * rows_dev)),
             dma((2, 2, 2, max(UP, DOWN))),
             dma((rows_dev + 2,)),
         ],
@@ -607,7 +669,7 @@
     paired = offset_bias.shape[1] % 8 == 0 and 2 * HEAD_DIM == 128 and 2 * GRID_W == 128
     square = lax.axis_size("tp") == 4 and offset_bias.shape[1] * HEAD_DIM == residual.shape[1]
     rows_dev = residual.shape[0] // GRID_W
-    even = lax.axis_size("sp") % 2 == 0 and rows_dev == ATTEND
+    even = lax.axis_size("sp") % 2 == 0 and rows_dev == 2 * (AHEAD - 1)
     body = generic_device
     if paired and square and even:
         body = square_device

time: 109 us -> 103 us (0.945)
  Pallas kernels: 106 us -> 101 us
    pallas_call x1, Pallas kernels: 106 us -> 101 us  [square_device(): pl.pallas_call(lambda *refs: stack_kernel(rows_dev, needs, *refs), out_sh...]
where the time goes in v2:
time: 103 us
  Pallas kernels  101 us (98%)
  local copies, waits for them, and re-layouts  1.77 us (2%)
    pallas_call x1, Pallas kernels, square_device(): pl.pallas_call(lambda *refs: stack_kernel(rows_dev, needs, *refs), out_sh...  101 us

profile of v2, /device:TPU:8, one launch (start us, length us, event | category | flops | bytes accessed | tf_op | source)
XLA Modules:
  0.0 102.5 jit_solution(11506165929363909151)
XLA Ops:
  0.0 100.8 %stack.1 = bf16[384,512]{1,0:T(8,128)(2,1)} custom-call(bf16[384,512]{1,0:T(8,128)(2,1)} %refs_0_.1, bf16[3,512]{1,0:T(4,128)(2,1)} %refs_1_.1, f32[3,15,8,31]{3,2,1,0:T(8,128)} %bitcast.1, bf16[3,512,2048]{2,1,0:T(8,128)(2,1)} %refs_3_.1, bf16[3,512,2048]{2,1,0:T(8,128)(2,1)} %refs_4_.1, bf16[3,512,2048]{2,1,0:T(8,128)(2,1)} %refs_5_.1, ...), custom_call_target="tpu_custom_call" | custom-call | tf_op jit(solution)/shard_map/stack/pallas_call | solution.py:636
  100.8 1.8 %copy.9 = bf16[384,512]{1,0:T(8,128)(2,1)} copy(bf16[384,512]{1,0:T(8,128)(2,1)} %stack.1) | data formatting | bytes 786432

commit v3 on v2

--- a/solution.py
+++ b/solution.py
@@ -281,7 +281,7 @@
 def stack_kernel(
     rows_dev, needs,
     x_ref, gain_ref, bias_ref, wq_ref, wk_ref, wv_ref, wo_ref, out_ref,
-    gains, weights, stream, mixed, keyval, queries, scaled, squares, sums, tables, bias, partial,
+    gains, weights, stream, mixed, keyval, queries, scaled, squares, own_squares, sums, parts, tables, bias, partial,
     weight_sems, gain_sems, stream_sems, mixed_sems, halo_sems, local_sems,
 ):
     sp, sp_size = lax.axis_index("sp"), lax.axis_size("sp")
@@ -391,26 +391,37 @@
             def _():
                 streams.send(index + AHEAD)
 
+    def own_rows(layer):
+        source, folded = scale_slot(layer, me, slice(None))
+        for kind in range(3):
+            weight_copy(kind, layer).wait()
+            whole = project(layer, me, kind, source)
+            for chunk in range(rows_dev // 2):
+                sums[chunk, kind] = whole[chunk * TALL : (chunk + 1) * TALL]
+        for chunk in range(rows_dev // 2):
+            own_squares[chunk] = folded[chunk * TALL : (chunk + 1) * TALL]
+
+    def place_of(chunk):
+        return chunk + even * (rows_dev // 2 - 1 - 2 * chunk)
+
     def start_rows(layer, chunk, kind):
-        here = pair_at(chunk)
-        slots = (me, across, over)
+        here, place = pair_at(chunk), place_of(chunk)
+        slots = (across, over)
         if kind == 0:
             folded = jnp.zeros((TALL, 128), jnp.float32)
-            for place, slot in enumerate(slots):
-                scaled[chunk, place], square = scale_slot(layer, slot, here)
+            for turn, slot in enumerate(slots):
+                scaled[chunk, turn], square = scale_slot(layer, slot, here)
                 folded += square
             squares[chunk] = folded
-        if chunk == 0:
-            weight_copy(kind, layer).wait()
-        sums[chunk, kind] = sum(
-            project(layer, slot, kind, scaled[chunk, place]) for place, slot in enumerate(slots)
+        parts[chunk, kind] = sum(
+            project(layer, slot, kind, scaled[chunk, turn]) for turn, slot in enumerate(slots)
         )
 
     def end_rows(layer, chunk, part):
-        here, parity = pair_at(chunk), layer % 2
+        here, place, parity = pair_at(chunk), place_of(chunk), layer % 2
         if part == 1:
             queries[here, :] = (
-                (sums[chunk, 2] + project(layer, corner, 2, scaled[chunk, 3]))
+                (sums[place, 2] + parts[chunk, 2] + project(layer, corner, 2, scaled[chunk, 2]))
                 * (squares[chunk, :, :1] * (HEAD_DIM ** (-0.5) * LOG2E))
             ).astype(jnp.bfloat16)
             return
@@ -418,14 +429,15 @@
         for index in rows:
             streams.finish(index)
         source, folded = scale_slot(layer, corner, here)
-        scaled[chunk, 3] = source
-        total = jnp.sum(squares[chunk] + folded, axis=1, keepdims=True)
+        scaled[chunk, 2] = source
+        total = jnp.sum(own_squares[place] + squares[chunk] + folded, axis=1, keepdims=True)
         inverse = lax.rsqrt(total * (1.0 / total_feats) + epsilon)
         squares[chunk] = jnp.broadcast_to(inverse, (TALL, 128))
         there = pl.ds(pl.multiple_of(here.start + UP * GRID_W, GRID_W), TALL)
         for kind in range(2):
             keyval[parity, there, kind * width : (kind + 1) * width] = (
-                (sums[chunk, kind] + project(layer, corner, kind, source)) * inverse
+                (sums[place, kind] + parts[chunk, kind] + project(layer, corner, kind, source))
+                * inverse
             ).astype(jnp.bfloat16)
         for index in rows:
             row = row_of(index)
@@ -438,11 +450,10 @@
             def _(row=row):
                 halo_copy(parity, True, row - (rows_dev - UP)).start()
 
+    def next_tables(layer):
+        pl.when(layer < layers - 1)(lambda: make_tables(layer + 1))
+
     def make_tables(layer):
-        @pl.when(layer == 0)
-        def _():
-            load_bias.wait()
-
         low, high = pair_lanes(bias[layer])
         heads = bias.shape[2]
 
@@ -547,7 +558,7 @@
             store_out(chunk).start()
 
     plan = (
-        (make_tables, None),
+        (own_rows, None),
         (relay_stream, None, 0),
         (relay_stream, None, 1),
         (start_rows, None, 0, 0),
@@ -558,25 +569,23 @@
         (start_rows, None, 1, 0),
         (start_rows, None, 1, 1),
         (start_rows, None, 1, 2),
-        (end_rows, None, 0, 0),
         (relay_stream, None, 4),
-        (end_rows, None, 0, 1),
-        (end_rows, None, 1, 0),
         (relay_stream, None, 5),
         (start_rows, None, 2, 0),
         (start_rows, None, 2, 1),
+        (end_rows, None, 0, 0),
+        (end_rows, None, 1, 0),
+        (end_rows, None, 2, 0),
+        (end_rows, None, 0, 1),
         (start_rows, None, 2, 2),
+        (end_rows, None, 2, 1),
         (end_rows, None, 1, 1),
-        (end_rows, None, 2, 0),
-        (attend, early, 0, 0),
-        (attend, early, 0, 1),
-        (end_rows, None, 2, 1),
-        (attend, ~early, 0, 0),
-        (attend, ~early, 0, 1),
+        (attend, None, 0, 0),
+        (attend, None, 0, 1),
         (attend, None, 1, 0),
         (attend, None, 1, 1),
         (attend, None, 2, 0),
-        (attend, None, 2, 1),
+        (attend, ~early, 2, 1),
         (attend, ~early, 3, 0),
         (attend, ~early, 3, 1),
         (attend, ~early, 4, 0),
@@ -586,15 +595,16 @@
         (relay_mixed, None, 0, 0),
         (relay_mixed, None, 0, 1),
         (relay_mixed, None, 1, 0),
-        (relay_mixed, None, 1, 1),
-        (relay_mixed, None, 2, 0),
+        (attend, early, 2, 1),
         (attend, early, 3, 0),
         (attend, early, 3, 1),
         (attend, early, 4, 0),
         (attend, early, 4, 1),
         (attend, early, 5, 0),
         (attend, early, 5, 1),
+        (relay_mixed, None, 1, 1),
         (start_mixed, None, 0),
+        (relay_mixed, None, 2, 0),
         (relay_mixed, None, 2, 1),
         (relay_mixed, None, 3, 0),
         (relay_mixed, None, 3, 1),
@@ -603,8 +613,9 @@
         (relay_mixed, None, 4, 1),
         (relay_mixed, None, 5, 0),
         (relay_mixed, None, 5, 1),
+        (start_mixed, None, 2),
         (end_mixed, None, 0),
-        (start_mixed, None, 2),
+        (next_tables, None),
         (end_mixed, None, 1),
         (end_mixed, None, 2),
     )
@@ -617,6 +628,8 @@
                 pl.when(when)(lambda: step(layer, *place))
         return carry
 
+    load_bias.wait()
+    make_tables(0)
     lax.fori_loop(0, layers, one_layer, 0)
     for index in range(rows_dev):
         mixes.drain(index)
@@ -645,8 +658,10 @@
             pltpu.VMEM((4, tokens, feats), bf16),
             pltpu.VMEM((2, padded, 2 * feats), bf16),
             pltpu.VMEM((tokens, feats), bf16),
-            pltpu.VMEM((rows_dev // 2, 4, TALL, feats), bf16),
+            pltpu.VMEM((rows_dev // 2, 3, TALL, feats), bf16),
             pltpu.VMEM((rows_dev // 2, TALL, 128), f32),
+            pltpu.VMEM((rows_dev // 2, TALL, 128), f32),
+            pltpu.VMEM((rows_dev // 2, 3, TALL, feats), f32),
             pltpu.VMEM((rows_dev // 2, 3, TALL, feats), f32),
             pltpu.VMEM((feats // 128, row_offs * GRID_W, 128), f32),
             pltpu.VMEM((layers, row_offs, heads, col_offs), f32),

time: 103 us -> 101 us (0.981)
  Pallas kernels: 101 us -> 99.3 us
    pallas_call x1, Pallas kernels: 101 us -> 99.3 us  [square_device(): pl.pallas_call(lambda *refs: stack_kernel(rows_dev, needs, *refs), out_sh...]
where the time goes in v3:
time: 101 us
  Pallas kernels  99.3 us (98%)
  local copies, waits for them, and re-layouts  1.77 us (2%)
    pallas_call x1, Pallas kernels, square_device(): pl.pallas_call(lambda *refs: stack_kernel(rows_dev, needs, *refs), out_sh...  99.3 us

profile of v3, /device:TPU:8, one launch (start us, length us, event | category | flops | bytes accessed | tf_op | source)
XLA Modules:
  0.0 101.0 jit_solution(16372973308331710605)
XLA Ops:
  0.0 99.3 %stack.1 = bf16[384,512]{1,0:T(8,128)(2,1)} custom-call(bf16[384,512]{1,0:T(8,128)(2,1)} %refs_0_.1, bf16[3,512]{1,0:T(4,128)(2,1)} %refs_1_.1, f32[3,15,8,31]{3,2,1,0:T(8,128)} %bitcast.1, bf16[3,512,2048]{2,1,0:T(8,128)(2,1)} %refs_3_.1, bf16[3,512,2048]{2,1,0:T(8,128)(2,1)} %refs_4_.1, bf16[3,512,2048]{2,1,0:T(8,128)(2,1)} %refs_5_.1, ...), custom_call_target="tpu_custom_call" | custom-call | tf_op jit(solution)/shard_map/stack/pallas_call | solution.py:649
  99.3 1.8 %copy.9 = bf16[384,512]{1,0:T(8,128)(2,1)} copy(bf16[384,512]{1,0:T(8,128)(2,1)} %stack.1) | data formatting | bytes 786432

commit v4 on v3

--- a/solution.py
+++ b/solution.py
@@ -281,7 +281,7 @@
 def stack_kernel(
     rows_dev, needs,
     x_ref, gain_ref, bias_ref, wq_ref, wk_ref, wv_ref, wo_ref, out_ref,
-    gains, weights, stream, mixed, keyval, queries, scaled, squares, own_squares, sums, parts, tables, bias, partial,
+    gains, weights, stream, mixed, keyval, queries, scaled, squares, own_squares, sums, parts, tables, bias, own_gain, partial,
     weight_sems, gain_sems, stream_sems, mixed_sems, halo_sems, local_sems,
 ):
     sp, sp_size = lax.axis_index("sp"), lax.axis_size("sp")
@@ -312,7 +312,9 @@
 
     load_x = pltpu.make_async_copy(x_ref, stream.at[me], local_sems.at[rows_dev])
     load_bias = pltpu.make_async_copy(bias_ref, bias, local_sems.at[rows_dev + 1])
+    load_gain = pltpu.make_async_copy(gain_ref, own_gain, local_sems.at[rows_dev + 2])
     load_x.start()
+    load_gain.start()
     load_bias.start()
 
     barrier = pltpu.get_barrier_semaphore()
@@ -331,7 +333,8 @@
         for kind in range(4):
             weight_copy(kind, layer).start()
 
-    gains[me, 0:layers, :] = gain_ref[...].astype(jnp.float32)
+    load_gain.wait()
+    gains[me, 0:layers, :] = own_gain[...].astype(jnp.float32)
     sides = jnp.minimum(sp, 1) + jnp.minimum(sp_size - 1 - sp, 1)
     load_x.wait()
     pl.semaphore_wait(barrier, 3 + sides)
@@ -339,10 +342,11 @@
     def gain_copy(index, slot, peer):
         return tp_copy(gains.at[slot], gains.at[slot], gain_sems, index, peer)
 
-    for index, peer in enumerate((across, over, corner)):
-        gain_copy(index, me, peer).start()
     for index in range(AHEAD):
         streams.send(index)
+        if index == 0:
+            for place, peer in enumerate((across, over, corner)):
+                gain_copy(place, me, peer).start()
 
     def halo_copy(parity, up, k):
         local = rows_dev - UP + k if up else k
@@ -521,13 +525,13 @@
 
     def relay_mixed(layer, index, half):
         mixes.relay(index, half)
+        if index == 0 and half == 0:
+            weight_copy(3, layer).wait()
 
     def start_mixed(layer, chunk):
         here = pair_at(chunk)
         for index in (2 * chunk, 2 * chunk + 1):
             mixes.settle(index)
-        if chunk == 0:
-            weight_copy(3, layer).wait()
         total = stream[me, here, :].astype(jnp.float32)
         for slot in (me, across, over):
             total += project(layer, slot, 3, mixed[slot, here, :])
@@ -561,31 +565,31 @@
         (own_rows, None),
         (relay_stream, None, 0),
         (relay_stream, None, 1),
+        (relay_stream, None, 2),
         (start_rows, None, 0, 0),
-        (start_rows, None, 0, 1),
-        (start_rows, None, 0, 2),
-        (relay_stream, None, 2),
         (relay_stream, None, 3),
         (start_rows, None, 1, 0),
         (start_rows, None, 1, 1),
         (start_rows, None, 1, 2),
+        (start_rows, None, 0, 1),
+        (start_rows, None, 0, 2),
         (relay_stream, None, 4),
         (relay_stream, None, 5),
+        (end_rows, None, 0, 0),
+        (end_rows, None, 1, 0),
         (start_rows, None, 2, 0),
         (start_rows, None, 2, 1),
-        (end_rows, None, 0, 0),
-        (end_rows, None, 1, 0),
         (end_rows, None, 2, 0),
         (end_rows, None, 0, 1),
+        (end_rows, None, 1, 1),
         (start_rows, None, 2, 2),
         (end_rows, None, 2, 1),
-        (end_rows, None, 1, 1),
         (attend, None, 0, 0),
         (attend, None, 0, 1),
         (attend, None, 1, 0),
         (attend, None, 1, 1),
         (attend, None, 2, 0),
-        (attend, ~early, 2, 1),
+        (attend, None, 2, 1),
         (attend, ~early, 3, 0),
         (attend, ~early, 3, 1),
         (attend, ~early, 4, 0),
@@ -595,29 +599,28 @@
         (relay_mixed, None, 0, 0),
         (relay_mixed, None, 0, 1),
         (relay_mixed, None, 1, 0),
-        (attend, early, 2, 1),
+        (relay_mixed, None, 1, 1),
+        (relay_mixed, None, 2, 0),
         (attend, early, 3, 0),
         (attend, early, 3, 1),
         (attend, early, 4, 0),
         (attend, early, 4, 1),
         (attend, early, 5, 0),
         (attend, early, 5, 1),
-        (relay_mixed, None, 1, 1),
-        (start_mixed, None, 0),
-        (relay_mixed, None, 2, 0),
         (relay_mixed, None, 2, 1),
         (relay_mixed, None, 3, 0),
         (relay_mixed, None, 3, 1),
         (start_mixed, None, 1),
         (relay_mixed, None, 4, 0),
+        (start_mixed, None, 0),
         (relay_mixed, None, 4, 1),
         (relay_mixed, None, 5, 0),
         (relay_mixed, None, 5, 1),
+        (end_mixed, None, 0),
         (start_mixed, None, 2),
-        (end_mixed, None, 0),
-        (next_tables, None),
         (end_mixed, None, 1),
         (end_mixed, None, 2),
+        (next_tables, None),
     )
 
     def one_layer(layer, carry):
@@ -641,7 +644,6 @@
     tokens, feats = residual.shape
     layers, heads, row_offs, col_offs = offset_bias.shape
     rows_dev = tokens // GRID_W
-    vmem = pl.BlockSpec(memory_space=pltpu.VMEM)
     hbm = pl.BlockSpec(memory_space=pl.ANY)
     bf16, f32, dma = jnp.bfloat16, jnp.float32, pltpu.SemaphoreType.DMA
     padded = tokens + (UP + DOWN) * GRID_W
@@ -649,7 +651,7 @@
     return pl.pallas_call(
         lambda *refs: stack_kernel(rows_dev, needs, *refs),
         out_shape=jax.ShapeDtypeStruct(residual.shape, bf16),
-        in_specs=[hbm, vmem] + [hbm] * 5,
+        in_specs=[hbm] * 7,
         out_specs=hbm,
         scratch_shapes=[
             pltpu.VMEM((4, -(-layers // 8) * 8, feats), f32),
@@ -665,13 +667,14 @@
             pltpu.VMEM((rows_dev // 2, 3, TALL, feats), f32),
             pltpu.VMEM((feats // 128, row_offs * GRID_W, 128), f32),
             pltpu.VMEM((layers, row_offs, heads, col_offs), f32),
+            pltpu.VMEM(norm_gain.shape, bf16),
             pltpu.VMEM((rows_dev // 2, TALL, feats), f32),
             dma((4, layers)),
             dma((2, 3)),
             dma((3, 2, 2 * rows_dev)),
             dma((3, 2, 2 * rows_dev)),
             dma((2, 2, 2, max(UP, DOWN))),
-            dma((rows_dev + 2,)),
+            dma((rows_dev + 3,)),
         ],
         compiler_params=pltpu.CompilerParams(
             collective_id=0, has_side_effects=True, vmem_limit_bytes=56 * 1024 * 1024

time: 101 us -> 99.6 us (0.986)
  Pallas kernels: 99.3 us -> 97.3 us
    pallas_call x1, Pallas kernels: 99.3 us -> 97.3 us  [square_device(): pl.pallas_call(lambda *refs: stack_kernel(rows_dev, needs, *refs), out_sh...]
where the time goes in v4:
time: 99.6 us; the launch traced here: 99.1 us
  Pallas kernels  97.3 us (98%)
  local copies, waits for them, and re-layouts  1.77 us (2%)
    pallas_call x1, Pallas kernels, square_device(): pl.pallas_call(lambda *refs: stack_kernel(rows_dev, needs, *refs), out_sh...  97.3 us

profile of v4, /device:TPU:8, one launch (start us, length us, event | category | flops | bytes accessed | tf_op | source)
XLA Modules:
  0.0 99.1 jit_solution(4992580040205137458)
XLA Ops:
  0.0 97.3 %stack.1 = bf16[384,512]{1,0:T(8,128)(2,1)} custom-call(bf16[384,512]{1,0:T(8,128)(2,1)} %refs_0_.1, bf16[3,512]{1,0:T(4,128)(2,1)} %refs_1_.1, f32[3,15,8,31]{3,2,1,0:T(8,128)} %bitcast.1, bf16[3,512,2048]{2,1,0:T(8,128)(2,1)} %refs_3_.1, bf16[3,512,2048]{2,1,0:T(8,128)(2,1)} %refs_4_.1, bf16[3,512,2048]{2,1,0:T(8,128)(2,1)} %refs_5_.1, ...), custom_call_target="tpu_custom_call" | custom-call | tf_op jit(solution)/shard_map/stack/pallas_call | solution.py:651
  97.3 1.8 %copy.9 = bf16[384,512]{1,0:T(8,128)(2,1)} copy(bf16[384,512]{1,0:T(8,128)(2,1)} %stack.1) | data formatting | bytes 786432
